TPU v7x, 32 devices: a whole 2x2x4 slice. The times are simulated.
32 devices in a mesh: grp: 2 (over y), sp: 4 (over z), tp: 4 (over x, core).
Axes of the slice: x: 2, y: 2, z: 4, core: 2. Of those that a mesh axis runs over, the one named last changes fastest.
Arguments:
- query_first: bfloat16 [1536, 512], P(('grp', 'sp'), 'tp'), parts along dimension 0, may hold values from -172 to 172
- key_first: bfloat16 [1536, 512], P(('grp', 'sp'), 'tp'), parts along dimension 0, may hold values from -7.8 to 7.8
- query_second: bfloat16 [1536, 1024], P(('grp', 'sp'), 'tp'), parts along dimension 0, may hold values from -172 to 172
- key_second: bfloat16 [1536, 1024], P(('grp', 'sp'), 'tp'), parts along dimension 0, may hold values from -7.8 to 7.8
- values: bfloat16 [1536, 2, 512], P(('grp', 'sp'), None, 'tp'), parts along dimension 0, may hold values from -6 to 6
- lambdas: float32 [2, 4], P(None, 'tp'), may hold values from 0.3 to 0.8
- residual: bfloat16 [1536, 2048], P(('grp', 'sp'), 'tp'), parts along dimension 0, may hold values from -130 to 130
- norm_gain: bfloat16 [2048], P('tp'), may hold values from 0.099609375 to 1.8984375
- out_weight: bfloat16 [2, 512, 2048], P(None, 'tp'), may hold values from -0.1875 to 0.1875
- gate_weight: bfloat16 [2048, 5632], P('sp', 'tp'), may hold values from -0.125 to 0.125
- up_weight: bfloat16 [2048, 5632], P('sp', 'tp'), may hold values from -0.125 to 0.125
- down_weight: bfloat16 [5632, 2048], P('tp', 'sp'), may hold values from -0.078125 to 0.078125
Outputs:
- layer_out: bfloat16 [1536, 2048], P(('grp', 'sp'), 'tp'), parts along dimension 0
There are 2 independent parts, one for each index of `grp`. A program takes and returns all parts, laid end to end along the dimension named above; an argument that names none is the same for every part. Nothing has to cross between parts.
All inputs are finite; a program needn't handle non-finite values.
Results may differ from a plain program's by a relative error of at most 0.0065.
Values may be sent and summed in bfloat16 or wider, within the bound.
A program may use at most 128 MiB of HBM per device.

v0:
```python
import jax
import jax.numpy as jnp
from jax import lax
from jax.sharding import PartitionSpec as P

D = 2048


def per_device(
    query_first,
    key_first,
    query_second,
    key_second,
    values,
    lambdas,
    residual,
    norm_gain,
    out_weight,
    gate_weight,
    up_weight,
    down_weight,
):
    tok_rows = query_first.shape[0]
    heads_here = lambdas.shape[1]
    width_first = query_first.shape[1] // (2 * heads_here)
    width_second = query_second.shape[1] // (2 * heads_here)
    value_size = values.shape[2] // heads_here
    offset = lax.axis_index("sp") * tok_rows
    query_pos = offset + lax.broadcasted_iota(jnp.int32, (tok_rows, 1), 0)
    query_groups = (
        query_first.reshape(tok_rows, heads_here, 2, width_first),
        query_second.reshape(tok_rows, heads_here, 2, width_second),
    )
    key_widths = (width_first, width_second)
    start_state = (
        jnp.full((heads_here, 2, tok_rows, 1), -1e30, jnp.float32),
        jnp.zeros((heads_here, 2, tok_rows, 1), jnp.float32),
        jnp.zeros((heads_here, 2, tok_rows, value_size), jnp.float32),
    )
    states = (start_state, start_state)
    pieces = (
        lax.all_gather(key_first, "sp", axis=0, tiled=True),
        lax.all_gather(key_second, "sp", axis=0, tiled=True),
        lax.all_gather(values, "sp", axis=0, tiled=True),
    )
    piece_rows = pieces[0].shape[0]
    key_pos = lax.broadcasted_iota(jnp.int32, (1, piece_rows), 1)
    allowed = key_pos <= query_pos
    value_rows = pieces[2].reshape(piece_rows, 2, heads_here, value_size)
    results = []
    for group_idx in range(2):
        key_width = key_widths[group_idx]
        key_part = pieces[group_idx].reshape(piece_rows, heads_here, 2, key_width)
        scores = jnp.einsum(
            "qhmd,khmd->hmqk", query_groups[group_idx], key_part, preferred_element_type=jnp.float32
        ) * key_width ** (-0.5)
        scores = jnp.where(allowed, scores, -1e30)
        running, totals, weighted = states[group_idx]
        new_peak = jnp.maximum(running, jnp.max(scores, axis=-1, keepdims=True))
        weights = jnp.where(allowed, jnp.exp(scores - new_peak), 0.0)
        totals = jnp.sum(weights, axis=-1, keepdims=True)
        weighted = jnp.einsum(
            "hmqk,khe->hmqe",
            weights.astype(jnp.bfloat16),
            value_rows[:, group_idx],
            preferred_element_type=jnp.float32,
        )
        results.append((new_peak, totals, weighted))
    states = (results[0], results[1])
    map_out = jnp.stack([states[0][2] / states[0][1], states[1][2] / states[1][1]])
    differ = map_out[:, :, 0] - lambdas[:, :, None, None] * map_out[:, :, 1]
    head_scale = lax.rsqrt(jnp.mean(differ * differ, axis=-1, keepdims=True) + 1e-06)
    attended = (0.8 * differ * head_scale).astype(jnp.bfloat16)
    projection = out_weight.reshape(2, heads_here, value_size, out_weight.shape[2])
    mixed_part = jnp.einsum(
        "ghqe,gher->qr", attended, projection, preferred_element_type=jnp.float32
    )
    mixed = lax.psum_scatter(
        mixed_part.astype(jnp.bfloat16), "tp", scatter_dimension=1, tiled=True
    ).astype(jnp.float32)
    stream = residual.astype(jnp.float32) + mixed
    squares = lax.psum(jnp.sum(stream * stream, axis=1), "tp")
    row_scale = lax.rsqrt(squares[:, None] / D + 1e-06)
    normed = (stream * row_scale * norm_gain.astype(jnp.float32)).astype(jnp.bfloat16)
    full_rows = lax.all_gather(normed, "tp", axis=1, tiled=True)
    pieces = (
        lax.all_gather(gate_weight, "sp", axis=0, tiled=True),
        lax.all_gather(up_weight, "sp", axis=0, tiled=True),
    )
    gate = jnp.dot(full_rows, pieces[0], preferred_element_type=jnp.float32)
    up_part = jnp.dot(full_rows, pieces[1], preferred_element_type=jnp.float32)
    hidden = (jax.nn.silu(gate) * up_part).astype(jnp.bfloat16)
    partial_out = jnp.dot(
        hidden,
        lax.all_gather(down_weight, "sp", axis=1, tiled=True),
        preferred_element_type=jnp.float32,
    )
    ffn = lax.psum_scatter(
        partial_out.astype(jnp.bfloat16), "tp", scatter_dimension=1, tiled=True
    ).astype(jnp.float32)
    return (stream + 0.5 * ffn).astype(jnp.bfloat16)


def solution(mesh):
    return jax.shard_map(
        per_device,
        mesh=mesh,
        in_specs=(
            P(("grp", "sp"), "tp"),
            P(("grp", "sp"), "tp"),
            P(("grp", "sp"), "tp"),
            P(("grp", "sp"), "tp"),
            P(("grp", "sp"), None, "tp"),
            P(None, "tp"),
            P(("grp", "sp"), "tp"),
            P("tp"),
            P(None, "tp", None),
            P("sp", "tp"),
            P("sp", "tp"),
            P("tp", "sp"),
        ),
        out_specs=P(("grp", "sp"), "tp"),
        check_vma=False,
    )
```

profile of v0, /device:TPU:0, one launch (start us, length us, event | category | flops | bytes accessed | tf_op | source)
XLA Modules:
  0.0 419.4 jit_solution(9682786560967322755)
XLA Ops:
  7.6 16.6 %all_gather.23 = bf16[768,256]{1,0:T(8,128)(2,1)S(1)} all-gather(bf16[192,256]{1,0:T(8,128)(2,1)} %param.15), channel_id=1, replica_groups=mesh['grp'=2,'sp'=4,'tp'=4] {'sp'}, dimensions={0}, use_global_device_ids=true | all-gather | bytes 491520 | tf_op jit(solution)/shard_map/all_gather | solution.py:43
  24.4 14.4 %all_gather.21 = bf16[768,128]{1,0:T(8,128)(2,1)S(1)} all-gather(bf16[192,128]{1,0:T(8,128)(2,1)S(1)} %copy-done.6), channel_id=1, replica_groups=mesh['grp'=2,'sp'=4,'tp'=4] {'sp'}, dimensions={0}, use_global_device_ids=true | all-gather | bytes 245760 | tf_op jit(solution)/shard_map/all_gather | solution.py:42
  39.1 14.8 %all_gather.22 = bf16[768,2,128]{2,0,1:T(8,128)(2,1)S(1)} all-gather(bf16[192,2,128]{2,0,1:T(8,128)(2,1)S(1)} %copy.27), channel_id=1, replica_groups=mesh['grp'=2,'sp'=4,'tp'=4] {'sp'}, dimensions={0}, use_global_device_ids=true | all-gather | bytes 491520 | tf_op jit(solution)/shard_map/all_gather | solution.py:44
  53.8 0.5 fusion.34
  54.3 0.5 fusion.35
  54.8 0.7 fusion.6
  55.5 0.4 fusion.5
  55.9 0.4 fusion.4
  56.8 1.3 fusion
  58.3 0.5 all-gather.4.cloned.1.call-update
  58.9 0.5 all-gather.6.cloned.1.call-update
  59.4 0.5 all-gather.8.cloned.1.call-update
  60.0 22.8 %reduce-scatter.3.cloned.1.call-done = bf16[192,512]{1,0:T(8,128)(2,1)} async-done(((bf16[192,2048]{1,0:T(8,128)(2,1)}), bf16[192,512]{1,0:T(8,128)(2,1)}) %reduce-scatter.3.cloned.1.call-update) | async-done | bytes 196624 | tf_op jit(solution)/shard_map/reduce_scatter | solution.py:78
  82.8 1.1 multiply_reduce_fusion
  83.9 6.1 %psum.7 = f32[192]{0:T(256)S(1)} all-reduce(f32[192]{0:T(256)S(1)} %multiply_reduce_fusion), channel_id=1, replica_groups=mesh['grp'=2,'sp'=4,'tp'=4] {'tp'}, use_global_device_ids=true, to_apply=%region_7.8 | all-reduce | flops 192 | bytes 1536 | tf_op jit(solution)/shard_map/psum | solution.py:82
  90.0 1.0 multiply_convert_fusion
  91.0 8.4 %all_gather.24 = bf16[192,2048]{1,0:T(8,128)(2,1)S(1)} all-gather(bf16[192,512]{1,0:T(8,128)(2,1)S(1)} %multiply_convert_fusion), channel_id=1, replica_groups=mesh['grp'=2,'sp'=4,'tp'=4] {'tp'}, dimensions={1}, use_global_device_ids=true | all-gather | bytes 983040 | tf_op jit(solution)/shard_map/all_gather | solution.py:85
  99.4 68.7 %all-gather.4.cloned.1.call-done = bf16[2048,1408]{1,0:T(8,128)(2,1)} async-done(((bf16[512,1408]{1,0:T(8,128)(2,1)}), bf16[2048,1408]{1,0:T(8,128)(2,1)}) %all-gather.4.cloned.1.call-update) | async-done | bytes 5767184 | tf_op jit(solution)/shard_map/all_gather | solution.py:87
  168.1 4.0 fusion.36
  172.1 102.2 %all-gather.6.cloned.1.call-done = bf16[2048,1408]{1,0:T(8,128)(2,1)} async-done(((bf16[512,1408]{1,0:T(8,128)(2,1)}), bf16[2048,1408]{1,0:T(8,128)(2,1)}) %all-gather.6.cloned.1.call-update) | async-done | bytes 5767184 | tf_op jit(solution)/shard_map/all_gather | solution.py:88
  274.4 106.3 %all-gather.8.cloned.1.call-done = bf16[1408,2048]{1,0:T(8,128)(2,1)} async-done(((bf16[1408,512]{1,0:T(8,128)(2,1)}), bf16[1408,2048]{1,0:T(8,128)(2,1)}) %all-gather.8.cloned.1.call-update) | async-done | bytes 5767184 | tf_op jit(solution)/shard_map/all_gather | solution.py:95
  380.6 7.9 %convolution_convert_fusion = bf16[192,2048]{1,0:T(8,128)(2,1)} fusion(bf16[1408,2048]{1,0:T(8,128)(2,1)} %all-gather.8.cloned.1.call-done, bf16[192,2048]{1,0:T(8,128)(2,1)S(1)} %all_gather.24, bf16[2048,1408]{1,0:T(8,128)(2,1)} %all-gather.6.cloned.1.call-done, f32[192,1408]{1,0:T(8,128)S(1)} %fusion.36), kind=kOutput, calls=%fused_computation.4 | convolution fusion | flops 2216607744 | bytes 14188544 | tf_op jit(solution)/shard_map/dot_general | solution.py:93
  388.5 21.6 %reduce-scatter.5.cloned.1.call-done = bf16[192,512]{1,0:T(8,128)(2,1)} async-done(((bf16[192,2048]{1,0:T(8,128)(2,1)}), bf16[192,512]{1,0:T(8,128)(2,1)}) %reduce-scatter.5.cloned.1.call-update) | async-done | bytes 196624 | tf_op jit(solution)/shard_map/reduce_scatter | solution.py:98
  410.2 1.7 add_convert_fusion
  (36 shorter events, 1.3 us)
Async XLA Ops:
  7.4 49.5 %copy-start = (bf16[2,128,2048]{2,1,0:T(8,128)(2,1)S(1)}, bf16[2,128,2048]{2,1,0:T(8,128)(2,1)}, u32[]{:S(2)}) copy-start(bf16[2,128,2048]{2,1,0:T(8,128)(2,1)} %param.20) | copy-start | bytes 3145732
  7.4 17.0 %copy-start.6 = (bf16[192,128]{1,0:T(8,128)(2,1)S(1)}, bf16[192,128]{1,0:T(8,128)(2,1)}, u32[]{:S(2)}) copy-start(bf16[192,128]{1,0:T(8,128)(2,1)} %param.13) | copy-start | bytes 147460
  7.4 31.5 %copy-start.5 = (bf16[192,128]{1,0:T(8,128)(2,1)S(1)}, bf16[192,128]{1,0:T(8,128)(2,1)}, u32[]{:S(2)}) copy-start(bf16[192,128]{1,0:T(8,128)(2,1)} %param.12) | copy-start | bytes 147460
  7.4 31.7 %copy-start.4 = (bf16[192,2,128]{2,1,0:T(2,128)(2,1)S(1)}, bf16[192,2,128]{2,1,0:T(2,128)(2,1)}, u32[]{:S(2)}) copy-start(bf16[192,2,128]{2,1,0:T(2,128)(2,1)} %param.16) | copy-start | bytes 294916
  7.4 75.4 %reduce-scatter.3.cloned.1.call-start = ((), (), s32[]{:S(2)}) async-start(), calls=%async_computation.2 | async-start | bytes 983040 | tf_op jit(solution)/shard_map/reduce_scatter | solution.py:78
  24.2 29.6 %copy-start.3 = (bf16[192,256]{1,0:T(8,128)(2,1)S(1)}, bf16[192,256]{1,0:T(8,128)(2,1)}, u32[]{:S(2)}) copy-start(bf16[192,256]{1,0:T(8,128)(2,1)} %param.14) | copy-start | bytes 294916
  55.9 0.7 copy-start.7
  58.2 109.9 %all-gather.4.cloned.1.call-start = ((), (), s32[]{:S(2)}) async-start(), calls=%async_computation.3 | async-start | bytes 7208960 | tf_op jit(solution)/shard_map/all_gather | solution.py:87
  58.8 1.2 copy-start.8
  58.8 24.0 %copy-start.1 = (bf16[192,512]{1,0:T(8,128)(2,1)S(1)}, bf16[192,512]{1,0:T(8,128)(2,1)}, u32[]{:S(2)}) copy-start(bf16[192,512]{1,0:T(8,128)(2,1)} %param.18) | copy-start | bytes 589828
  58.8 215.6 %all-gather.6.cloned.1.call-start = ((), (), s32[]{:S(2)}) async-start(), calls=%async_computation.4 | async-start | bytes 7208960 | tf_op jit(solution)/shard_map/all_gather | solution.py:88
  59.4 321.3 %all-gather.8.cloned.1.call-start = ((), (), s32[]{:S(2)}) async-start(), calls=%async_computation.5 | async-start | bytes 7208960 | tf_op jit(solution)/shard_map/all_gather | solution.py:95
  60.0 350.2 %reduce-scatter.5.cloned.1.call-start = ((), (), s32[]{:S(2)}) async-start(), calls=%async_computation.6 | async-start | bytes 983040 | tf_op jit(solution)/shard_map/reduce_scatter | solution.py:98
  172.1 238.0 %copy-start.2 = (bf16[192,512]{1,0:T(8,128)(2,1)S(1)}, bf16[192,512]{1,0:T(8,128)(2,1)}, u32[]{:S(2)}) copy-start(bf16[192,512]{1,0:T(8,128)(2,1)} %reduce-scatter.3.cloned.1.call-done) | copy-start | bytes 589828
Sparse Core Ops, SparseCore 0:
  58.3 24.4 reduce-scatter.2
  388.7 21.4 reduce-scatter.4
Sparse Core Ops, SparseCore 1:
  60.3 107.8 all-gather.3
  169.5 104.8 all-gather.5
  275.8 104.8 all-gather.7
where the time goes:
time: 420 us; the launch traced here: 419 us
  waiting for transfers between devices  323 us (77%)
  blocking collectives  60.2 us (14%)
  between operations  15.2 us (4%)
  matrix products  15.1 us (4%)
  other arithmetic  4.87 us (1%)
    all_gather x1, waiting for transfers between devices, per_device(): lax.all_gather(down_weight, 'sp', axis=1, tiled=True)  106 us
    all_gather x1, waiting for transfers between devices, per_device(): lax.all_gather(up_weight, 'sp', axis=0, tiled=True)  102 us
    all_gather x1, waiting for transfers between devices, per_device(): lax.all_gather(gate_weight, 'sp', axis=0, tiled=True)  68.7 us
    reduce_scatter x1, waiting for transfers between devices, per_device(): lax.psum_scatter(mixed_part.astype(jnp.bfloat16), 'tp', scatter_dimension...  22.8 us
    reduce_scatter x1, waiting for transfers between devices, per_device(): lax.psum_scatter(partial_out.astype(jnp.bfloat16), 'tp', scatter_dimensio...  21.6 us
    all_gather x1, blocking collectives, per_device(): lax.all_gather(key_second, 'sp', axis=0, tiled=True)  16.6 us
    all_gather x1, blocking collectives, per_device(): lax.all_gather(values, 'sp', axis=0, tiled=True)  14.8 us
    all_gather x1, blocking collectives, per_device(): lax.all_gather(key_first, 'sp', axis=0, tiled=True)  14.4 us
  transfers between devices with their start and end apart: 5, of which 5 were waited for; matrix products, arithmetic and copies ran while one was open for 1% of the time, Pallas kernels for 0%

commit v1 on v0

--- a/solution.py
+++ b/solution.py
@@ -4,6 +4,17 @@
 from jax.sharding import PartitionSpec as P
 
 D = 2048
+
+
+def ring_gather(x, axis, dim):
+    ways = lax.axis_size(axis)
+    pieces = [x]
+    for far in range(1, ways):
+        pieces.append(
+            lax.ppermute(pieces[far - 1], axis, [(d, (d - 1) % ways) for d in range(ways)])
+        )
+    line = jnp.concatenate(pieces, axis=dim)
+    return jnp.roll(line, lax.axis_index(axis) * x.shape[dim], axis=dim)
 
 
 def per_device(
@@ -91,9 +102,7 @@
     up_part = jnp.dot(full_rows, pieces[1], preferred_element_type=jnp.float32)
     hidden = (jax.nn.silu(gate) * up_part).astype(jnp.bfloat16)
     partial_out = jnp.dot(
-        hidden,
-        lax.all_gather(down_weight, "sp", axis=1, tiled=True),
-        preferred_element_type=jnp.float32,
+        hidden, ring_gather(down_weight, "sp", 1), preferred_element_type=jnp.float32
     )
     ffn = lax.psum_scatter(
         partial_out.astype(jnp.bfloat16), "tp", scatter_dimension=1, tiled=True

time: 420 us -> 388 us (0.924)
  waiting for transfers between devices: 323 us -> 268 us
  local copies, waits for them, and re-layouts: 0.68 us -> 19.5 us
    ppermute x0 -> x3, waiting for transfers between devices: none -> 154 us  [ring_gather(): lax.ppermute(pieces[far - 1], axis, [(d, (d - 1) % ways) for d in range(w...]
    all_gather x1 -> x0, waiting for transfers between devices: 106 us -> none  [per_device(): lax.all_gather(down_weight, 'sp', axis=1, tiled=True)]
    all_gather x1, waiting for transfers between devices: 68.7 us -> 0.01 us  [per_device(): lax.all_gather(gate_weight, 'sp', axis=0, tiled=True)]
    reduce_scatter x1, waiting for transfers between devices: 22.8 us -> 0.01 us  [per_device(): lax.psum_scatter(mixed_part.astype(jnp.bfloat16), 'tp', scatter_dimension...]
    unnamed x20 -> x29, local copies, waits for them, and re-layouts: 0.37 us -> 16.3 us
    all_gather x1, waiting for transfers between devices: 102 us -> 92 us  [per_device(): lax.all_gather(up_weight, 'sp', axis=0, tiled=True)]
  transfers between devices with their start and end apart: 5 -> 7, of which waited for: 5 -> 5; matrix products, arithmetic and copies ran while one was open for 1% -> 6% of each run, Pallas kernels for 0% -> 0%
where the time goes in v1:
time: 388 us; the launch traced here: 387 us
  waiting for transfers between devices  268 us (69%)
  blocking collectives  60.4 us (16%)
  local copies, waits for them, and re-layouts  19.5 us (5%)
  matrix products  15.3 us (4%)
  between operations  15 us (4%)
  other arithmetic  4.89 us (1%)
    ppermute x3, waiting for transfers between devices, ring_gather(): lax.ppermute(pieces[far - 1], axis, [(d, (d - 1) % ways) for d in range(w...  154 us
    all_gather x1, waiting for transfers between devices, per_device(): lax.all_gather(up_weight, 'sp', axis=0, tiled=True)  92 us
    reduce_scatter x1, waiting for transfers between devices, per_device(): lax.psum_scatter(partial_out.astype(jnp.bfloat16), 'tp', scatter_dimensio...  21.6 us
    all_gather x1, blocking collectives, per_device(): lax.all_gather(key_second, 'sp', axis=0, tiled=True)  16.6 us
    unnamed x29, local copies, waits for them, and re-layouts  16.3 us
    all_gather x1, blocking collectives, per_device(): lax.all_gather(values, 'sp', axis=0, tiled=True)  14.8 us
    all_gather x1, blocking collectives, per_device(): lax.all_gather(key_first, 'sp', axis=0, tiled=True)  14.4 us
    all_gather x1, blocking collectives, per_device(): full_rows = lax.all_gather(normed, 'tp', axis=1, tiled=True)  8.6 us
  transfers between devices with their start and end apart: 7, of which 5 were waited for; matrix products, arithmetic and copies ran while one was open for 6% of the time, Pallas kernels for 0%

profile of v1, /device:TPU:0, one launch (start us, length us, event | category | flops | bytes accessed | tf_op | source)
XLA Modules:
  0.0 387.1 jit_solution(781363093430632308)
XLA Ops:
  7.4 16.6 %all_gather.20 = bf16[768,256]{1,0:T(8,128)(2,1)S(1)} all-gather(bf16[192,256]{1,0:T(8,128)(2,1)} %param.15), channel_id=1, replica_groups=mesh['grp'=2,'sp'=4,'tp'=4] {'sp'}, dimensions={0}, use_global_device_ids=true | all-gather | bytes 491520 | tf_op jit(solution)/shard_map/all_gather | solution.py:54
  24.5 14.4 %all_gather.18 = bf16[768,128]{1,0:T(8,128)(2,1)S(1)} all-gather(bf16[192,128]{1,0:T(8,128)(2,1)S(1)} %copy-done.7), channel_id=1, replica_groups=mesh['grp'=2,'sp'=4,'tp'=4] {'sp'}, dimensions={0}, use_global_device_ids=true | all-gather | bytes 245760 | tf_op jit(solution)/shard_map/all_gather | solution.py:53
  39.1 14.8 %all_gather.19 = bf16[768,2,128]{2,0,1:T(8,128)(2,1)S(1)} all-gather(bf16[192,2,128]{2,0,1:T(8,128)(2,1)S(1)} %copy.27), channel_id=1, replica_groups=mesh['grp'=2,'sp'=4,'tp'=4] {'sp'}, dimensions={0}, use_global_device_ids=true | all-gather | bytes 491520 | tf_op jit(solution)/shard_map/all_gather | solution.py:55
  56.9 1.3 fusion.2
  59.6 3.5 collective-permute-start
  63.1 75.4 %collective-permute-done = bf16[1408,512]{1,0:T(8,128)(2,1)} collective-permute-done((bf16[1408,512]{1,0:T(8,128)(2,1)S(1)}, bf16[1408,512]{1,0:T(8,128)(2,1)}, u32[]{:S(2)}, u32[]{:S(2)}) %collective-permute-start) | collective-permute-done | bytes 1441824 | tf_op jit(solution)/shard_map/ppermute | solution.py:14
  138.5 1.3 constant_dynamic-update-slice_fusion.7
  139.8 77.4 %collective-permute-done.1 = bf16[1408,512]{1,0:T(8,128)(2,1)} collective-permute-done((bf16[1408,512]{1,0:T(8,128)(2,1)}, bf16[1408,512]{1,0:T(8,128)(2,1)}, u32[]{:S(2)}, u32[]{:S(2)}) %collective-permute-start.1) | collective-permute-done | bytes 1441824 | tf_op jit(solution)/shard_map/ppermute | solution.py:14
  217.2 2.7 constant_dynamic-update-slice_fusion.6
  219.8 1.1 multiply_reduce_fusion
  220.9 6.1 %psum.7 = f32[192]{0:T(256)S(1)} all-reduce(f32[192]{0:T(256)S(1)} %multiply_reduce_fusion), channel_id=1, replica_groups=mesh['grp'=2,'sp'=4,'tp'=4] {'tp'}, use_global_device_ids=true, to_apply=%region_7.8 | all-reduce | flops 192 | bytes 1536 | tf_op jit(solution)/shard_map/psum | solution.py:93
  227.0 1.0 multiply_convert_fusion
  228.0 8.6 %all_gather.21 = bf16[192,2048]{1,0:T(8,128)(2,1)S(1)} all-gather(bf16[192,512]{1,0:T(8,128)(2,1)S(1)} %multiply_convert_fusion), channel_id=1, replica_groups=mesh['grp'=2,'sp'=4,'tp'=4] {'tp'}, dimensions={1}, use_global_device_ids=true | all-gather | bytes 983040 | tf_op jit(solution)/shard_map/all_gather | solution.py:96
  236.6 2.7 constant_dynamic-update-slice_fusion.5
  240.1 2.6 constant_dynamic-update-slice_fusion.4
  242.7 1.2 constant_dynamic-update-slice_fusion.3
  244.0 2.6 constant_dynamic-update-slice_fusion.2
  246.6 2.7 constant_dynamic-update-slice_fusion.1
  249.3 2.9 constant_dynamic-update-slice_fusion
  252.1 4.3 %fusion.42 = f32[192,1408]{1,0:T(8,128)S(1)} fusion(bf16[192,2048]{1,0:T(8,128)(2,1)S(1)} %all_gather.21, bf16[2048,1408]{1,0:T(8,128)(2,1)} %all-gather.3.cloned.1.call-done), kind=kOutput, calls=%fused_computation.71 | convolution fusion | flops 1107296256 | bytes 7634944 | tf_op jit(solution)/shard_map/dot_general | solution.py:101
  256.4 92.0 %all-gather.5.cloned.1.call-done = bf16[2048,1408]{1,0:T(8,128)(2,1)} async-done(((bf16[512,1408]{1,0:T(8,128)(2,1)}), bf16[2048,1408]{1,0:T(8,128)(2,1)}) %all-gather.5.cloned.1.call-update) | async-done | bytes 5767184 | tf_op jit(solution)/shard_map/all_gather | solution.py:99
  348.4 7.9 %fusion.4 = bf16[192,2048]{1,0:T(8,128)(2,1)} fusion(bf16[1408,4096]{1,0:T(8,128)(2,1)} %constant_dynamic-update-slice_fusion, s32[]{:T(128)S(6)} %select_n.35, bf16[192,2048]{1,0:T(8,128)(2,1)S(1)} %all_gather.21, bf16[2048,1408]{1,0:T(8,128)(2,1)} %all-gather.5.cloned.1.call-done, f32[192,1408]{1,0:T(8,128)S(1)} %fusion.42), kind=kOutput, calls=%fused_computation.6 | convolution fusion | flops 2216607744 | bytes 14188548 | tf_op jit(solution)/shard_map/dot_general | solution.py:104
  356.3 21.6 %reduce-scatter.5.cloned.1.call-done = bf16[192,512]{1,0:T(8,128)(2,1)} async-done(((bf16[192,2048]{1,0:T(8,128)(2,1)}), bf16[192,512]{1,0:T(8,128)(2,1)}) %reduce-scatter.5.cloned.1.call-update) | async-done | bytes 196624 | tf_op jit(solution)/shard_map/reduce_scatter | solution.py:107
  378.0 1.7 add_convert_fusion
  (49 shorter events, 5.8 us)
Async XLA Ops:
  7.4 49.5 %copy-start = (bf16[2,128,2048]{2,1,0:T(8,128)(2,1)S(1)}, bf16[2,128,2048]{2,1,0:T(8,128)(2,1)}, u32[]{:S(2)}) copy-start(bf16[2,128,2048]{2,1,0:T(8,128)(2,1)} %param.20) | copy-start | bytes 3145732
  7.4 17.0 %copy-start.6 = (bf16[192,128]{1,0:T(8,128)(2,1)S(1)}, bf16[192,128]{1,0:T(8,128)(2,1)}, u32[]{:S(2)}) copy-start(bf16[192,128]{1,0:T(8,128)(2,1)} %param.12) | copy-start | bytes 147460
  7.4 17.1 %copy-start.7 = (bf16[192,128]{1,0:T(8,128)(2,1)S(1)}, bf16[192,128]{1,0:T(8,128)(2,1)}, u32[]{:S(2)}) copy-start(bf16[192,128]{1,0:T(8,128)(2,1)} %param.13) | copy-start | bytes 147460
  7.4 31.7 %copy-start.5 = (bf16[192,2,128]{2,1,0:T(2,128)(2,1)S(1)}, bf16[192,2,128]{2,1,0:T(2,128)(2,1)}, u32[]{:S(2)}) copy-start(bf16[192,2,128]{2,1,0:T(2,128)(2,1)} %param.16) | copy-start | bytes 294916
  7.4 46.5 %copy-start.4 = (bf16[192,256]{1,0:T(8,128)(2,1)S(1)}, bf16[192,256]{1,0:T(8,128)(2,1)}, u32[]{:S(2)}) copy-start(bf16[192,256]{1,0:T(8,128)(2,1)} %param.14) | copy-start | bytes 294916
  7.4 212.5 %reduce-scatter.3.cloned.1.call-start = ((), (), s32[]{:S(2)}) async-start(), calls=%async_computation.2 | async-start | bytes 983040 | tf_op jit(solution)/shard_map/reduce_scatter | solution.py:89
  56.0 0.7 copy-start.8
  58.2 1.4 copy-start.1
  58.2 80.2 %copy-start.9 = (bf16[512]{0:T(512)(128)(2,1)S(1)}, bf16[512]{0:T(512)(128)(2,1)}, u32[]{:S(2)}) copy-start(bf16[512]{0:T(512)(128)(2,1)} %param.19) | copy-start | bytes 3076
  58.3 193.9 %all-gather.3.cloned.1.call-start = ((), (), s32[]{:S(2)}) async-start(), calls=%async_computation.3 | async-start | bytes 7208960 | tf_op jit(solution)/shard_map/all_gather | solution.py:98
  58.8 289.6 %all-gather.5.cloned.1.call-start = ((), (), s32[]{:S(2)}) async-start(), calls=%async_computation.4 | async-start | bytes 7208960 | tf_op jit(solution)/shard_map/all_gather | solution.py:99
  59.4 318.5 %reduce-scatter.5.cloned.1.call-start = ((), (), s32[]{:S(2)}) async-start(), calls=%async_computation.5 | async-start | bytes 983040 | tf_op jit(solution)/shard_map/reduce_scatter | solution.py:107
  59.6 78.9 %collective-permute-start = (bf16[1408,512]{1,0:T(8,128)(2,1)S(1)}, bf16[1408,512]{1,0:T(8,128)(2,1)}, u32[]{:S(2)}, u32[]{:S(2)}) collective-permute-start(bf16[1408,512]{1,0:T(8,128)(2,1)S(1)} %copy-done.1), channel_id=1, source_target_pairs={{0,12},{4,0},{8,4},{12,8},{1,13},{5,1},{9,5},{13,9},{2,14},{6,2},{... | collective-permute-start | bytes 4325384 | tf_op jit(solution)/shard_map/ppermute | solution.py:14
  138.5 78.7 %collective-permute-start.1 = (bf16[1408,512]{1,0:T(8,128)(2,1)}, bf16[1408,512]{1,0:T(8,128)(2,1)}, u32[]{:S(2)}, u32[]{:S(2)}) collective-permute-start(bf16[1408,512]{1,0:T(8,128)(2,1)} %collective-permute-done), channel_id=1, source_target_pairs={{0,12},{4,0},{8,4},{12,8},{1,13},{5,1},{9,5},{13,9},{2,14},{6,2},{... | collective-permute-start | bytes 4325384 | tf_op jit(solution)/shard_map/ppermute | solution.py:14
  139.8 80.0 %copy-start.2 = (bf16[192,512]{1,0:T(8,128)(2,1)S(1)}, bf16[192,512]{1,0:T(8,128)(2,1)}, u32[]{:S(2)}) copy-start(bf16[192,512]{1,0:T(8,128)(2,1)} %param.18) | copy-start | bytes 589828
  217.2 22.9 %collective-permute-start.2 = (bf16[1408,512]{1,0:T(8,128)(2,1)}, bf16[1408,512]{1,0:T(8,128)(2,1)}, u32[]{:S(2)}, u32[]{:S(2)}) collective-permute-start(bf16[1408,512]{1,0:T(8,128)(2,1)} %collective-permute-done.1), channel_id=1, source_target_pairs={{0,12},{4,0},{8,4},{12,8},{1,13},{5,1},{9,5},{13,9},{2,14},{6,2},{... | collective-permute-start | bytes 4325384 | tf_op jit(solution)/shard_map/ppermute | solution.py:14
  256.4 121.6 %copy-start.3 = (bf16[192,512]{1,0:T(8,128)(2,1)S(1)}, bf16[192,512]{1,0:T(8,128)(2,1)}, u32[]{:S(2)}) copy-start(bf16[192,512]{1,0:T(8,128)(2,1)} %reduce-scatter.3.cloned.1.call-done) | copy-start | bytes 589828
Sparse Core Ops, SparseCore 0:
  58.4 24.3 reduce-scatter.2
  356.4 21.4 reduce-scatter.4
Sparse Core Ops, SparseCore 1:
  60.3 162.1 all-gather.2
  223.9 124.5 all-gather.4
